TPU v7x, 32 devices: a whole 2x2x4 slice. The times are simulated.
32 devices in a mesh: sp: 8 (over z, y), tp: 4 (over x, core).
Axes of the slice: x: 2, y: 2, z: 4, core: 2. Of those that a mesh axis runs over, the one named last changes fastest.
Arguments:
- residual_in: bfloat16 [6144, 2048], P('sp', 'tp'), may hold values from -11 to 11
- queries: bfloat16 [6144, 1024], P('sp', 'tp'), may hold values from -6 to 6
- keys: bfloat16 [6144, 256], P('sp'), may hold values from -6 to 6
- values: bfloat16 [6144, 256], P('sp'), may hold values from -6 to 6
- query_gain: float32 [128], replicated, may hold values from 1.5 to 5
- key_norm_gain: float32 [128], replicated, may hold values from 1.5 to 5
- out_weight: bfloat16 [1024, 2048], P('tp'), may hold values from -0.1875 to 0.1875
- mlp_gain: float32 [2048], replicated, may hold values from 0.1 to 1.9
- gate_weight: bfloat16 [2048, 5632], P('sp', 'tp'), may hold values from -0.125 to 0.125
- up_weight: bfloat16 [2048, 5632], P('sp', 'tp'), may hold values from -0.125 to 0.125
- down_weight: bfloat16 [5632, 2048], P('tp', 'sp'), may hold values from -0.15625 to 0.15625
Outputs:
- layer_out: bfloat16 [6144, 2048], P('sp', 'tp')
All inputs are finite; a program needn't handle non-finite values.
Results may differ from a plain program's by a relative error of at most 0.012.
The roundings to bfloat16 on the way count: a program that leaves them out, or rounds other values in their place, can miss the bound.
Values may be sent and summed in bfloat16 or wider, within the bound.
No kernel may reach another device: no remote copies, remote signals or barrier semaphores. Data moves between devices by JAX's collectives and lax.ppermute only.
A program may use at most 64 MiB of HBM per device.

v0:
```python
import jax
import jax.numpy as jnp
from jax import lax
from jax.sharding import PartitionSpec as P

D = 2048
HEAD_SIZE = 128
QUERY_HEADS = 8
KEY_VALUE_HEADS = 2
GRID = 64
eps = 1e-06
rotary_base = 10000.0


def apply_rotary(vectors, grid_positions):
    half_size = vectors.shape[-1] // 2
    frequency = rotary_base ** (-jnp.arange(0, half_size, 2, dtype=jnp.float32) / half_size)
    grid_row = (grid_positions // GRID).astype(jnp.float32)
    grid_col = (grid_positions % GRID).astype(jnp.float32)
    angles = jnp.concatenate(
        [grid_row[:, None] * frequency, grid_col[:, None] * frequency], axis=-1
    )[:, None, :]
    cosine_table = jnp.cos(angles)
    sine_table = jnp.sin(angles)
    first_half = vectors[..., :half_size]
    second_half = vectors[..., half_size:]
    return jnp.concatenate(
        [
            first_half * cosine_table - second_half * sine_table,
            first_half * sine_table + second_half * cosine_table,
        ],
        axis=-1,
    )


def per_head_norm(vectors, gain):
    return vectors * lax.rsqrt(jnp.mean(vectors * vectors, axis=-1, keepdims=True) + eps) * gain


def on_device(
    residual_in,
    queries,
    keys,
    values,
    query_gain,
    key_norm_gain,
    out_weight,
    mlp_gain,
    gate_weight,
    up_weight,
    down_weight,
):
    local_rows = residual_in.shape[0]
    local_heads = queries.shape[1] // HEAD_SIZE
    queries_per_group = QUERY_HEADS // KEY_VALUE_HEADS
    tp_index = lax.axis_index("tp")
    grid_positions = lax.axis_index("sp") * local_rows + jnp.arange(local_rows, dtype=jnp.int32)
    query_rows = apply_rotary(
        per_head_norm(
            queries.astype(jnp.float32).reshape(local_rows, local_heads, HEAD_SIZE), query_gain
        ),
        grid_positions,
    ).astype(jnp.bfloat16)
    query_matrix = jnp.transpose(query_rows, (1, 0, 2)).reshape(local_heads * local_rows, HEAD_SIZE)
    shared = tp_index * local_heads // queries_per_group
    own_keys = lax.dynamic_slice_in_dim(keys, shared * HEAD_SIZE, HEAD_SIZE, 1)
    own_values = lax.dynamic_slice_in_dim(values, shared * HEAD_SIZE, HEAD_SIZE, 1)
    key_matrix = apply_rotary(
        per_head_norm(own_keys.astype(jnp.float32)[:, None, :], key_norm_gain), grid_positions
    )[:, 0, :].astype(jnp.bfloat16)
    score_scale = HEAD_SIZE ** (-0.5)
    query_count = local_heads * local_rows
    start_state = (
        jnp.full((query_count,), -1e30, jnp.float32),
        jnp.zeros((query_count,), jnp.float32),
        jnp.zeros((query_count, HEAD_SIZE), jnp.float32),
    )
    key_piece = lax.all_gather(key_matrix, "sp", axis=0, tiled=True)
    value_piece = lax.all_gather(own_values, "sp", axis=0, tiled=True)
    piece_rows = key_piece.shape[0]
    block_count = -(-piece_rows // 2048)
    while piece_rows % block_count:
        block_count += 1
    block_width = piece_rows // block_count

    def one_block(block_index, state_inner):
        running_max, running_sum, weighted = state_inner
        block_keys = lax.dynamic_slice_in_dim(key_piece, block_index * block_width, block_width, 0)
        block_values = lax.dynamic_slice_in_dim(
            value_piece, block_index * block_width, block_width, 0
        )
        scores = (
            jnp.dot(query_matrix, block_keys.T, preferred_element_type=jnp.float32) * score_scale
        )
        new_max = jnp.maximum(running_max, jnp.max(scores, axis=1))
        factor = jnp.exp(running_max - new_max)
        weights = jnp.exp(scores - new_max[:, None])
        running_sum = running_sum * factor + jnp.sum(weights, axis=1)
        weighted = weighted * factor[:, None] + jnp.dot(
            weights.astype(jnp.bfloat16), block_values, preferred_element_type=jnp.float32
        )
        return (new_max, running_sum, weighted)

    running_max, running_sum, weighted = lax.fori_loop(0, block_count, one_block, start_state)
    attended = (weighted / running_sum[:, None]).astype(jnp.bfloat16)
    attended = jnp.transpose(
        attended.reshape(local_heads, local_rows, HEAD_SIZE), (1, 0, 2)
    ).reshape(local_rows, local_heads * HEAD_SIZE)
    own_width = residual_in.shape[1]
    projected = jnp.dot(attended, out_weight, preferred_element_type=jnp.float32).astype(
        jnp.bfloat16
    )
    share = lax.psum_scatter(projected, "tp", scatter_dimension=1, tiled=True).astype(jnp.float32)
    residual_mid = residual_in.astype(jnp.float32) + share
    squares = lax.psum(jnp.sum(residual_mid * residual_mid, axis=1), "tp")
    gain_own = lax.dynamic_slice_in_dim(mlp_gain, tp_index * own_width, own_width, 0)
    normed_own = (residual_mid * lax.rsqrt(squares / D + eps)[:, None] * gain_own).astype(
        jnp.bfloat16
    )
    normed = lax.all_gather(normed_own, "tp", axis=1, tiled=True)
    gate_out = jnp.dot(
        normed,
        lax.all_gather(gate_weight, "sp", axis=0, tiled=True),
        preferred_element_type=jnp.float32,
    )
    up_out = jnp.dot(
        normed,
        lax.all_gather(up_weight, "sp", axis=0, tiled=True),
        preferred_element_type=jnp.float32,
    )
    hidden = (jax.nn.silu(gate_out) * up_out).astype(jnp.bfloat16)
    down_terms = jnp.dot(
        hidden,
        lax.all_gather(down_weight, "sp", axis=1, tiled=True),
        preferred_element_type=jnp.float32,
    )
    down_share = lax.psum_scatter(
        down_terms.astype(jnp.bfloat16), "tp", scatter_dimension=1, tiled=True
    ).astype(jnp.float32)
    return (residual_mid + 0.5 * down_share).astype(jnp.bfloat16)


def solution(mesh):
    in_specs = (
        P("sp", "tp"),
        P("sp", "tp"),
        P("sp", None),
        P("sp", None),
        P(),
        P(),
        P("tp", None),
        P(),
        P("sp", "tp"),
        P("sp", "tp"),
        P("tp", "sp"),
    )
    out_specs = P("sp", "tp")
    return jax.shard_map(
        on_device, mesh=mesh, in_specs=in_specs, out_specs=out_specs, check_vma=False
    )
```

profile of v0, /device:TPU:0, one launch (start us, length us, event | category | flops | bytes accessed | tf_op | source)
XLA Modules:
  0.0 573.1 jit_solution(10254005252952721331)
XLA Ops:
  9.2 1.8 subtract_convert_fusion.1
  12.8 1.4 reshape.236
  14.1 1.7 fusion.18
  17.8 1.4 subtract_convert_fusion
  20.3 38.6 %all-gather.18.cloned.1.call-done = bf16[6144,1,128]{2,0,1:T(8,128)(2,1)} async-done(((bf16[768,1,128]{2,0,1:T(8,128)(2,1)}), bf16[6144,1,128]{2,0,1:T(8,128)(2,1)}) %all-gather.18.cloned.1.call-update) | async-done | bytes 1572880 | tf_op jit(solution)/shard_map/all_gather | solution.py:78
  58.9 44.8 %all-gather.8.cloned.1.call-done = bf16[6144,128]{1,0:T(8,128)(2,1)} async-done(((bf16[768,128]{1,0:T(8,128)(2,1)}), bf16[6144,128]{1,0:T(8,128)(2,1)}) %all-gather.8.cloned.1.call-update) | async-done | bytes 1572880 | tf_op jit(solution)/shard_map/all_gather | solution.py:79
  103.7 57.6 %while.18 = (s32[]{:T(128)}, f32[1536]{0:T(1024)S(1)}, f32[1536]{0:T(1024)S(1)}, f32[1536,128]{1,0:T(8,128)S(1)}, bf16[6144,128]{1,0:T(8,128)(2,1)}, /*index=5*/...) while((s32[]{:T(128)}, f32[1536]{0:T(1024)S(1)}, ...), condition=%wide.region_5.6_spmd.clone, body=%wide.region_2.5_spmd.clone.sunk | while | flops 1636376064 | bytes 91193544 | solution.py:104
  103.7 7.4 %multiply_reduce_fusion.4 = (f32[1536]{0:T(1024)S(1)}, f32[2048,1536]{1,0:T(8,128)}) fusion(bf16[1536,128]{1,0:T(8,128)(2,1)S(1)} %get-tuple-element.266, bf16[6144,128]{1,0:T(8,128)(2,1)} %get-tuple-element.265, s32[]{:T(128)S(6)} %select_n.55), kind=kOutput, calls=%fused_computation.1.clone.1 | convolution fusion | flops 811596288 | bytes 13506564 | tf_op jit(solution)/shard_map/while/body/eval_jaxpr/dot_general | solution.py:93
  111.1 6.8 %fusion.49 = f32[1536]{0:T(1024)S(1)} fusion(f32[2048,1536]{1,0:T(8,128)} %get-tuple-element.236, f32[1536]{0:T(1024)S(1)} %select_maximum_fusion.2), kind=kLoop, calls=%fused_computation.3.clone.1 | loop fusion | flops 9435648 | bytes 12595200 | tf_op jit(solution)/shard_map/while/body/eval_jaxpr/reduce_sum | solution.py:98
  117.9 1.3 copy-done.1
  119.2 3.6 fusion.51
  122.9 7.4 %multiply_reduce_fusion.4 = (f32[1536]{0:T(1024)S(1)}, f32[2048,1536]{1,0:T(8,128)}) fusion(bf16[1536,128]{1,0:T(8,128)(2,1)S(1)} %get-tuple-element.266, bf16[6144,128]{1,0:T(8,128)(2,1)} %get-tuple-element.265, s32[]{:T(128)S(6)} %select_n.55), kind=kOutput, calls=%fused_computation.1.clone.1 | convolution fusion | flops 811596288 | bytes 13506564 | tf_op jit(solution)/shard_map/while/body/eval_jaxpr/dot_general | solution.py:93
  130.3 6.8 %fusion.49 = f32[1536]{0:T(1024)S(1)} fusion(f32[2048,1536]{1,0:T(8,128)} %get-tuple-element.236, f32[1536]{0:T(1024)S(1)} %select_maximum_fusion.2), kind=kLoop, calls=%fused_computation.3.clone.1 | loop fusion | flops 9435648 | bytes 12595200 | tf_op jit(solution)/shard_map/while/body/eval_jaxpr/reduce_sum | solution.py:98
  137.1 1.3 copy-done.1
  138.4 3.6 fusion.51
  142.1 7.4 %multiply_reduce_fusion.4 = (f32[1536]{0:T(1024)S(1)}, f32[2048,1536]{1,0:T(8,128)}) fusion(bf16[1536,128]{1,0:T(8,128)(2,1)S(1)} %get-tuple-element.266, bf16[6144,128]{1,0:T(8,128)(2,1)} %get-tuple-element.265, s32[]{:T(128)S(6)} %select_n.55), kind=kOutput, calls=%fused_computation.1.clone.1 | convolution fusion | flops 811596288 | bytes 13506564 | tf_op jit(solution)/shard_map/while/body/eval_jaxpr/dot_general | solution.py:93
  149.5 6.8 %fusion.49 = f32[1536]{0:T(1024)S(1)} fusion(f32[2048,1536]{1,0:T(8,128)} %get-tuple-element.236, f32[1536]{0:T(1024)S(1)} %select_maximum_fusion.2), kind=kLoop, calls=%fused_computation.3.clone.1 | loop fusion | flops 9435648 | bytes 12595200 | tf_op jit(solution)/shard_map/while/body/eval_jaxpr/reduce_sum | solution.py:98
  156.3 1.3 copy-done.1
  157.6 3.6 fusion.51
  161.8 2.7 convolution_convert_fusion
  166.1 34.7 %reduce-scatter.3.cloned.1.call-done = bf16[768,512]{1,0:T(8,128)(2,1)} async-done(((bf16[768,2048]{1,0:T(8,128)(2,1)}), bf16[768,512]{1,0:T(8,128)(2,1)}) %reduce-scatter.3.cloned.1.call-update) | async-done | bytes 786448 | tf_op jit(solution)/shard_map/reduce_scatter | solution.py:113
  200.8 1.5 multiply_reduce_fusion.1
  202.2 5.8 %psum.7 = f32[768]{0:T(1024)S(1)} all-reduce(f32[768]{0:T(1024)S(1)} %multiply_reduce_fusion.1), channel_id=1, replica_groups=mesh['sp'=8,'tp'=4] {'tp'}, use_global_device_ids=true, to_apply=%region_8.9 | all-reduce | flops 768 | bytes 6144 | tf_op jit(solution)/shard_map/psum | solution.py:115
  208.0 2.3 multiply_convert_fusion.1
  211.7 83.4 %all-gather.12.cloned.1.call-done = bf16[2048,1408]{1,0:T(8,128)(2,1)} async-done(((bf16[256,1408]{1,0:T(8,128)(2,1)}), bf16[2048,1408]{1,0:T(8,128)(2,1)}) %all-gather.12.cloned.1.call-update) | async-done | bytes 5767184 | tf_op jit(solution)/shard_map/all_gather | solution.py:123
  295.1 28.1 %all-gather.10.cloned.1.call-done = bf16[768,2048]{1,0:T(8,128)(2,1)} async-done(((bf16[768,512]{1,0:T(8,128)(2,1)}), bf16[768,2048]{1,0:T(8,128)(2,1)}) %all-gather.10.cloned.1.call-update) | async-done | bytes 3145744 | tf_op jit(solution)/shard_map/all_gather | solution.py:120
  323.3 9.7 %fusion.31 = f32[768,1408]{1,0:T(8,128)} fusion(bf16[768,2048]{1,0:T(8,128)(2,1)} %all-gather.10.cloned.1.call-done, bf16[2048,1408]{1,0:T(8,128)(2,1)} %all-gather.12.cloned.1.call-done), kind=kOutput, calls=%fused_computation.68 | convolution fusion | flops 4429185024 | bytes 13238272 | tf_op jit(solution)/shard_map/dot_general | solution.py:121
  333.0 84.7 %all-gather.14.cloned.1.call-done = bf16[2048,1408]{1,0:T(8,128)(2,1)} async-done(((bf16[256,1408]{1,0:T(8,128)(2,1)}), bf16[2048,1408]{1,0:T(8,128)(2,1)}) %all-gather.14.cloned.1.call-update) | async-done | bytes 5767184 | tf_op jit(solution)/shard_map/all_gather | solution.py:128
  417.6 93.4 %all-gather.16.cloned.1.call-done = bf16[1408,2048]{1,0:T(8,128)(2,1)} async-done(((bf16[1408,256]{1,0:T(8,128)(2,1)}), bf16[1408,2048]{1,0:T(8,128)(2,1)}) %all-gather.16.cloned.1.call-update) | async-done | bytes 5767184 | tf_op jit(solution)/shard_map/all_gather | solution.py:134
  511.0 16.8 %convolution_convert_fusion.1 = bf16[768,2048]{1,0:T(8,128)(2,1)} fusion(bf16[1408,2048]{1,0:T(8,128)(2,1)} %all-gather.16.cloned.1.call-done, f32[768,1408]{1,0:T(8,128)} %fusion.31, bf16[768,2048]{1,0:T(8,128)(2,1)} %all-gather.10.cloned.1.call-done, bf16[2048,1408]{1,0:T(8,128)(2,1)} %all-gather.14.cloned.1.call-done), kind=kOutput, calls=%fused_computation.19 | convolution fusion | flops 8866430976 | bytes 22151168 | tf_op jit(solution)/shard_map/dot_general | solution.py:132
  527.8 36.1 %reduce-scatter.5.cloned.1.call-done = bf16[768,512]{1,0:T(8,128)(2,1)} async-done(((bf16[768,2048]{1,0:T(8,128)(2,1)}), bf16[768,512]{1,0:T(8,128)(2,1)}) %reduce-scatter.5.cloned.1.call-update) | async-done | bytes 786448 | tf_op jit(solution)/shard_map/reduce_scatter | solution.py:137
  563.9 2.3 add_convert_fusion
  (58 shorter events, 10.8 us)
Async XLA Ops:
  6.5 155.2 %copy-start = (bf16[256,2048]{1,0:T(8,128)(2,1)S(1)}, bf16[256,2048]{1,0:T(8,128)(2,1)}, u32[]{:S(2)}) copy-start(bf16[256,2048]{1,0:T(8,128)(2,1)} %param.19) | copy-start | bytes 3145732
  6.5 5.4 copy-start.4
  6.5 52.4 %all-gather.18.cloned.1.call-start = ((), (), s32[]{:S(2)}) async-start(), calls=%async_computation.9 | async-start | bytes 1769472 | tf_op jit(solution)/shard_map/all_gather | solution.py:78
  9.2 7.5 %copy-start.5 = (f32[128]{0:T(128)S(1)}, f32[128]{0:T(128)}, u32[]{:S(2)}) copy-start(f32[128]{0:T(128)} %param.17) | copy-start | bytes 1540
  11.9 91.8 %all-gather.8.cloned.1.call-start = ((), (), s32[]{:S(2)}) async-start(), calls=%async_computation.2 | async-start | bytes 1769472 | tf_op jit(solution)/shard_map/all_gather | solution.py:79
  12.7 188.1 %reduce-scatter.3.cloned.1.call-start = ((), (), s32[]{:S(2)}) async-start(), calls=%async_computation.3 | async-start | bytes 3932160 | tf_op jit(solution)/shard_map/reduce_scatter | solution.py:113
  111.1 8.2 %copy-start.1 = (f32[2048,1536]{1,0:T(8,128)S(1)}, f32[2048,1536]{1,0:T(8,128)}, u32[]{:S(2)}) copy-start(f32[2048,1536]{1,0:T(8,128)} %get-tuple-element.236) | copy-start | bytes 37748740 | tf_op jit(solution)/shard_map/while
  130.3 8.2 %copy-start.1 = (f32[2048,1536]{1,0:T(8,128)S(1)}, f32[2048,1536]{1,0:T(8,128)}, u32[]{:S(2)}) copy-start(f32[2048,1536]{1,0:T(8,128)} %get-tuple-element.236) | copy-start | bytes 37748740 | tf_op jit(solution)/shard_map/while
  149.5 8.2 %copy-start.1 = (f32[2048,1536]{1,0:T(8,128)S(1)}, f32[2048,1536]{1,0:T(8,128)}, u32[]{:S(2)}) copy-start(f32[2048,1536]{1,0:T(8,128)} %get-tuple-element.236) | copy-start | bytes 37748740 | tf_op jit(solution)/shard_map/while
  161.8 39.0 %copy-start.2 = (bf16[768,512]{1,0:T(8,128)(2,1)S(1)}, bf16[768,512]{1,0:T(8,128)(2,1)}, u32[]{:S(2)}) copy-start(bf16[768,512]{1,0:T(8,128)(2,1)} %param.13) | copy-start | bytes 2359300
  164.5 130.6 %all-gather.12.cloned.1.call-start = ((), (), s32[]{:S(2)}) async-start(), calls=%async_computation.5 | async-start | bytes 6488064 | tf_op jit(solution)/shard_map/all_gather | solution.py:123
  165.1 158.2 %all-gather.10.cloned.1.call-start = ((), (), s32[]{:S(2)}) async-start(), calls=%async_computation.4 | async-start | bytes 3932160 | tf_op jit(solution)/shard_map/all_gather | solution.py:120
  210.3 207.3 %all-gather.14.cloned.1.call-start = ((), (), s32[]{:S(2)}) async-start(), calls=%async_computation.6 | async-start | bytes 6488064 | tf_op jit(solution)/shard_map/all_gather | solution.py:128
  210.9 300.1 %all-gather.16.cloned.1.call-start = ((), (), s32[]{:S(2)}) async-start(), calls=%async_computation.7 | async-start | bytes 6488064 | tf_op jit(solution)/shard_map/all_gather | solution.py:134
  211.7 352.2 %reduce-scatter.5.cloned.1.call-start = ((), (), s32[]{:S(2)}) async-start(), calls=%async_computation.8 | async-start | bytes 3932160 | tf_op jit(solution)/shard_map/reduce_scatter | solution.py:137
  333.0 230.9 %copy-start.3 = (bf16[768,512]{1,0:T(8,128)(2,1)S(1)}, bf16[768,512]{1,0:T(8,128)(2,1)}, u32[]{:S(2)}) copy-start(bf16[768,512]{1,0:T(8,128)(2,1)} %reduce-scatter.3.cloned.1.call-done) | copy-start | bytes 2359300
Sparse Core Ops, SparseCore 0:
  12.0 46.8 all-gather.17
  61.1 42.5 all-gather.7
  164.6 36.0 reduce-scatter.2
  202.8 92.2 all-gather.11
  296.5 26.6 all-gather.9
  325.3 92.3 all-gather.13
  419.7 91.2 all-gather.15
  527.9 35.8 reduce-scatter.4
where the time goes:
time: 574 us; the launch traced here: 573 us
  waiting for transfers between devices  446 us (78%)
  matrix products  62.2 us (11%)
  other arithmetic  38.3 us (7%)
  between operations  13.7 us (2%)
  local copies, waits for them, and re-layouts  7.03 us (1%)
  blocking collectives  5.77 us (1%)
    all_gather x1, waiting for transfers between devices, on_device(): lax.all_gather(down_weight, 'sp', axis=1, tiled=True)  93.4 us
    all_gather x1, waiting for transfers between devices, on_device(): lax.all_gather(up_weight, 'sp', axis=0, tiled=True)  84.7 us
    all_gather x1, waiting for transfers between devices, on_device(): lax.all_gather(gate_weight, 'sp', axis=0, tiled=True)  83.4 us
    all_gather x1, waiting for transfers between devices, on_device(): value_piece = lax.all_gather(own_values, 'sp', axis=0, tiled=True)  44.8 us
    all_gather x1, waiting for transfers between devices, on_device(): key_piece = lax.all_gather(key_matrix, 'sp', axis=0, tiled=True)  38.6 us
    reduce_scatter x1, waiting for transfers between devices, on_device(): lax.psum_scatter(down_terms.astype(jnp.bfloat16), 'tp', scatter_dimension...  36.1 us
    reduce_scatter x1, waiting for transfers between devices, on_device(): lax.psum_scatter(projected, 'tp', scatter_dimension=1, tiled=True)  34.7 us
    all_gather x1, waiting for transfers between devices, on_device(): normed = lax.all_gather(normed_own, 'tp', axis=1, tiled=True)  28.1 us
  transfers between devices with their start and end apart: 8, of which 8 were waited for; matrix products, arithmetic and copies ran while one was open for 4% of the time, Pallas kernels for 0%

commit v1 on v0

--- a/solution.py
+++ b/solution.py
@@ -76,7 +76,12 @@
         jnp.zeros((query_count, HEAD_SIZE), jnp.float32),
     )
     key_piece = lax.all_gather(key_matrix, "sp", axis=0, tiled=True)
-    value_piece = lax.all_gather(own_values, "sp", axis=0, tiled=True)
+    ring = [own_values]
+    for hop in range(7):
+        ring.append(lax.ppermute(ring[-1], "sp", [(dev, (dev + 1) % 8) for dev in range(8)]))
+    value_piece = jnp.roll(
+        jnp.concatenate(ring[::-1], axis=0), (lax.axis_index("sp") + 1) * ring[0].shape[0], axis=0
+    )
     piece_rows = key_piece.shape[0]
     block_count = -(-piece_rows // 2048)
     while piece_rows % block_count:

time: 574 us -> 556 us (0.969)
  waiting for transfers between devices: 446 us -> 416 us
  local copies, waits for them, and re-layouts: 7.03 us -> 15.9 us
    ppermute x0 -> x7, waiting for transfers between devices: none -> 50.2 us  [on_device(): lax.ppermute(ring[-1], 'sp', [(dev, (dev + 1) % 8) for dev in range(8)])]
    all_gather x1 -> x0, waiting for transfers between devices: 44.8 us -> none  [on_device(): value_piece = lax.all_gather(own_values, 'sp', axis=0, tiled=True)]
    all_gather x1, waiting for transfers between devices: 38.6 us -> 2.89 us  [on_device(): key_piece = lax.all_gather(key_matrix, 'sp', axis=0, tiled=True)]
    unnamed x10 -> x37, local copies, waits for them, and re-layouts: 0.02 us -> 6.96 us
  transfers between devices with their start and end apart: 8 -> 14, of which waited for: 8 -> 14; matrix products, arithmetic and copies ran while one was open for 4% -> 6% of each run, Pallas kernels for 0% -> 0%
where the time goes in v1:
time: 556 us; the launch traced here: 555 us
  waiting for transfers between devices  416 us (75%)
  matrix products  62.2 us (11%)
  other arithmetic  38.1 us (7%)
  local copies, waits for them, and re-layouts  15.9 us (3%)
  between operations  13.9 us (2%)
  blocking collectives  5.77 us (1%)
    all_gather x1, waiting for transfers between devices, on_device(): lax.all_gather(down_weight, 'sp', axis=1, tiled=True)  93.2 us
    all_gather x1, waiting for transfers between devices, on_device(): lax.all_gather(up_weight, 'sp', axis=0, tiled=True)  84.7 us
    all_gather x1, waiting for transfers between devices, on_device(): lax.all_gather(gate_weight, 'sp', axis=0, tiled=True)  83.5 us
    ppermute x7, waiting for transfers between devices, on_device(): lax.ppermute(ring[-1], 'sp', [(dev, (dev + 1) % 8) for dev in range(8)])  50.2 us
    reduce_scatter x1, waiting for transfers between devices, on_device(): lax.psum_scatter(down_terms.astype(jnp.bfloat16), 'tp', scatter_dimension...  36.1 us
    reduce_scatter x1, waiting for transfers between devices, on_device(): lax.psum_scatter(projected, 'tp', scatter_dimension=1, tiled=True)  35.1 us
    all_gather x1, waiting for transfers between devices, on_device(): normed = lax.all_gather(normed_own, 'tp', axis=1, tiled=True)  28.1 us
    dot_general x3, matrix products, one_block(): jnp.dot(query_matrix, block_keys.T, preferred_element_type=jnp.float32)  22.1 us
  transfers between devices with their start and end apart: 14, of which 14 were waited for; matrix products, arithmetic and copies ran while one was open for 6% of the time, Pallas kernels for 0%

profile of v1, /device:TPU:0, one launch (start us, length us, event | category | flops | bytes accessed | tf_op | source)
XLA Modules:
  0.0 555.0 jit_solution(7359884262307826526)
XLA Ops:
  7.6 3.0 collective-permute-start
  12.1 6.5 %collective-permute-done = bf16[768,128]{1,0:T(8,128)(2,1)S(1)} collective-permute-done((bf16[768,128]{1,0:T(8,128)(2,1)S(1)}, bf16[768,128]{1,0:T(8,128)(2,1)S(1)}, u32[]{:S(2)}, u32[]{:S(2)}) %collective-permute-start) | collective-permute-done | bytes 196640 | tf_op jit(solution)/shard_map/ppermute | solution.py:81
  19.7 7.6 %collective-permute-done.1 = bf16[768,128]{1,0:T(8,128)(2,1)S(1)} collective-permute-done((bf16[768,128]{1,0:T(8,128)(2,1)S(1)}, bf16[768,128]{1,0:T(8,128)(2,1)S(1)}, u32[]{:S(2)}, u32[]{:S(2)}) %collective-permute-start.1) | collective-permute-done | bytes 196640 | tf_op jit(solution)/shard_map/ppermute | solution.py:81
  27.3 1.8 subtract_convert_fusion.1
  29.1 6.6 %collective-permute-done.2 = bf16[768,128]{1,0:T(8,128)(2,1)S(1)} collective-permute-done((bf16[768,128]{1,0:T(8,128)(2,1)S(1)}, bf16[768,128]{1,0:T(8,128)(2,1)S(1)}, u32[]{:S(2)}, u32[]{:S(2)}) %collective-permute-start.2) | collective-permute-done | bytes 196640 | tf_op jit(solution)/shard_map/ppermute | solution.py:81
  38.8 5.2 collective-permute-done.3
  44.1 10.8 %collective-permute-done.4 = bf16[768,128]{1,0:T(8,128)(2,1)S(1)} collective-permute-done((bf16[768,128]{1,0:T(8,128)(2,1)S(1)}, bf16[768,128]{1,0:T(8,128)(2,1)S(1)}, u32[]{:S(2)}, u32[]{:S(2)}) %collective-permute-start.4) | collective-permute-done | bytes 196640 | tf_op jit(solution)/shard_map/ppermute | solution.py:81
  57.6 5.9 %collective-permute-done.5 = bf16[768,128]{1,0:T(8,128)(2,1)} collective-permute-done((bf16[768,128]{1,0:T(8,128)(2,1)S(1)}, bf16[768,128]{1,0:T(8,128)(2,1)}, u32[]{:S(2)}, u32[]{:S(2)}) %collective-permute-start.5) | collective-permute-done | bytes 196640 | tf_op jit(solution)/shard_map/ppermute | solution.py:81
  66.2 7.5 %collective-permute-done.6 = bf16[768,128]{1,0:T(8,128)(2,1)} collective-permute-done((bf16[768,128]{1,0:T(8,128)(2,1)}, bf16[768,128]{1,0:T(8,128)(2,1)}, u32[]{:S(2)}, u32[]{:S(2)}) %collective-permute-start.6) | collective-permute-done | bytes 196640 | tf_op jit(solution)/shard_map/ppermute | solution.py:81
  82.4 2.9 all-gather.15.cloned.1.call-done
  85.3 57.5 %while.18 = (s32[]{:T(128)}, f32[1536]{0:T(1024)S(1)}, f32[1536]{0:T(1024)S(1)}, f32[1536,128]{1,0:T(8,128)S(1)}, bf16[6144,128]{1,0:T(8,128)(2,1)}, /*index=5*/...) while((s32[]{:T(128)}, f32[1536]{0:T(1024)S(1)}, ...), condition=%wide.region_5.6_spmd.clone, body=%wide.region_2.5_spmd.clone.sunk | while | flops 1636376064 | bytes 91193544 | solution.py:109
  85.3 7.4 %multiply_reduce_fusion.4 = (f32[1536]{0:T(1024)S(1)}, f32[2048,1536]{1,0:T(8,128)}) fusion(bf16[1536,128]{1,0:T(8,128)(2,1)S(1)} %get-tuple-element.266, bf16[6144,128]{1,0:T(8,128)(2,1)} %get-tuple-element.265, s32[]{:T(128)S(6)} %select_n.69), kind=kOutput, calls=%fused_computation.1.clone.1 | convolution fusion | flops 811596288 | bytes 13506564 | tf_op jit(solution)/shard_map/while/body/eval_jaxpr/dot_general | solution.py:98
  92.6 6.8 %fusion.49 = f32[1536]{0:T(1024)S(1)} fusion(f32[2048,1536]{1,0:T(8,128)} %get-tuple-element.236, f32[1536]{0:T(1024)S(1)} %select_maximum_fusion.2), kind=kLoop, calls=%fused_computation.3.clone.1 | loop fusion | flops 9435648 | bytes 12595200 | tf_op jit(solution)/shard_map/while/body/eval_jaxpr/reduce_sum | solution.py:103
  100.8 3.6 fusion.51
  104.5 7.4 %multiply_reduce_fusion.4 = (f32[1536]{0:T(1024)S(1)}, f32[2048,1536]{1,0:T(8,128)}) fusion(bf16[1536,128]{1,0:T(8,128)(2,1)S(1)} %get-tuple-element.266, bf16[6144,128]{1,0:T(8,128)(2,1)} %get-tuple-element.265, s32[]{:T(128)S(6)} %select_n.69), kind=kOutput, calls=%fused_computation.1.clone.1 | convolution fusion | flops 811596288 | bytes 13506564 | tf_op jit(solution)/shard_map/while/body/eval_jaxpr/dot_general | solution.py:98
  111.8 6.8 %fusion.49 = f32[1536]{0:T(1024)S(1)} fusion(f32[2048,1536]{1,0:T(8,128)} %get-tuple-element.236, f32[1536]{0:T(1024)S(1)} %select_maximum_fusion.2), kind=kLoop, calls=%fused_computation.3.clone.1 | loop fusion | flops 9435648 | bytes 12595200 | tf_op jit(solution)/shard_map/while/body/eval_jaxpr/reduce_sum | solution.py:103
  120.0 3.6 fusion.51
  123.7 7.4 %multiply_reduce_fusion.4 = (f32[1536]{0:T(1024)S(1)}, f32[2048,1536]{1,0:T(8,128)}) fusion(bf16[1536,128]{1,0:T(8,128)(2,1)S(1)} %get-tuple-element.266, bf16[6144,128]{1,0:T(8,128)(2,1)} %get-tuple-element.265, s32[]{:T(128)S(6)} %select_n.69), kind=kOutput, calls=%fused_computation.1.clone.1 | convolution fusion | flops 811596288 | bytes 13506564 | tf_op jit(solution)/shard_map/while/body/eval_jaxpr/dot_general | solution.py:98
  131.0 6.8 %fusion.49 = f32[1536]{0:T(1024)S(1)} fusion(f32[2048,1536]{1,0:T(8,128)} %get-tuple-element.236, f32[1536]{0:T(1024)S(1)} %select_maximum_fusion.2), kind=kLoop, calls=%fused_computation.3.clone.1 | loop fusion | flops 9435648 | bytes 12595200 | tf_op jit(solution)/shard_map/while/body/eval_jaxpr/reduce_sum | solution.py:103
  139.2 3.6 fusion.51
  143.3 2.7 convolution_convert_fusion
  147.6 35.1 %reduce-scatter.3.cloned.1.call-done = bf16[768,512]{1,0:T(8,128)(2,1)} async-done(((bf16[768,2048]{1,0:T(8,128)(2,1)}), bf16[768,512]{1,0:T(8,128)(2,1)}) %reduce-scatter.3.cloned.1.call-update) | async-done | bytes 786448 | tf_op jit(solution)/shard_map/reduce_scatter | solution.py:118
  184.2 5.8 %psum.7 = f32[768]{0:T(1024)S(1)} all-reduce(f32[768]{0:T(1024)S(1)} %multiply_reduce_fusion.1), channel_id=1, replica_groups=mesh['sp'=8,'tp'=4] {'tp'}, use_global_device_ids=true, to_apply=%region_8.9 | all-reduce | flops 768 | bytes 6144 | tf_op jit(solution)/shard_map/psum | solution.py:120
  189.9 2.3 multiply_convert_fusion.1
  193.7 83.5 %all-gather.9.cloned.1.call-done = bf16[2048,1408]{1,0:T(8,128)(2,1)} async-done(((bf16[256,1408]{1,0:T(8,128)(2,1)}), bf16[2048,1408]{1,0:T(8,128)(2,1)}) %all-gather.9.cloned.1.call-update) | async-done | bytes 5767184 | tf_op jit(solution)/shard_map/all_gather | solution.py:128
  277.2 28.1 %all-gather.7.cloned.1.call-done = bf16[768,2048]{1,0:T(8,128)(2,1)} async-done(((bf16[768,512]{1,0:T(8,128)(2,1)}), bf16[768,2048]{1,0:T(8,128)(2,1)}) %all-gather.7.cloned.1.call-update) | async-done | bytes 3145744 | tf_op jit(solution)/shard_map/all_gather | solution.py:125
  305.4 9.7 %fusion.31 = f32[768,1408]{1,0:T(8,128)} fusion(bf16[768,2048]{1,0:T(8,128)(2,1)} %all-gather.7.cloned.1.call-done, bf16[2048,1408]{1,0:T(8,128)(2,1)} %all-gather.9.cloned.1.call-done), kind=kOutput, calls=%fused_computation.85 | convolution fusion | flops 4429185024 | bytes 13238272 | tf_op jit(solution)/shard_map/dot_general | solution.py:126
  315.1 84.7 %all-gather.11.cloned.1.call-done = bf16[2048,1408]{1,0:T(8,128)(2,1)} async-done(((bf16[256,1408]{1,0:T(8,128)(2,1)}), bf16[2048,1408]{1,0:T(8,128)(2,1)}) %all-gather.11.cloned.1.call-update) | async-done | bytes 5767184 | tf_op jit(solution)/shard_map/all_gather | solution.py:133
  399.7 93.2 %all-gather.13.cloned.1.call-done = bf16[1408,2048]{1,0:T(8,128)(2,1)} async-done(((bf16[1408,256]{1,0:T(8,128)(2,1)}), bf16[1408,2048]{1,0:T(8,128)(2,1)}) %all-gather.13.cloned.1.call-update) | async-done | bytes 5767184 | tf_op jit(solution)/shard_map/all_gather | solution.py:139
  493.0 16.8 %convolution_convert_fusion.1 = bf16[768,2048]{1,0:T(8,128)(2,1)} fusion(bf16[1408,2048]{1,0:T(8,128)(2,1)} %all-gather.13.cloned.1.call-done, f32[768,1408]{1,0:T(8,128)} %fusion.31, bf16[768,2048]{1,0:T(8,128)(2,1)} %all-gather.7.cloned.1.call-done, bf16[2048,1408]{1,0:T(8,128)(2,1)} %all-gather.11.cloned.1.call-done), kind=kOutput, calls=%fused_computation.19 | convolution fusion | flops 8866430976 | bytes 22151168 | tf_op jit(solution)/shard_map/dot_general | solution.py:137
  509.8 36.1 %reduce-scatter.5.cloned.1.call-done = bf16[768,512]{1,0:T(8,128)(2,1)} async-done(((bf16[768,2048]{1,0:T(8,128)(2,1)}), bf16[768,512]{1,0:T(8,128)(2,1)}) %reduce-scatter.5.cloned.1.call-update) | async-done | bytes 786448 | tf_op jit(solution)/shard_map/reduce_scatter | solution.py:142
  545.8 2.3 add_convert_fusion
  (98 shorter events, 29.3 us)
Async XLA Ops:
  6.5 136.8 %copy-start = (bf16[256,2048]{1,0:T(8,128)(2,1)S(1)}, bf16[256,2048]{1,0:T(8,128)(2,1)}, u32[]{:S(2)}) copy-start(bf16[256,2048]{1,0:T(8,128)(2,1)} %param.19) | copy-start | bytes 3145732
  6.5 78.7 %all-gather.15.cloned.1.call-start = ((), (), s32[]{:S(2)}) async-start(), calls=%async_computation.8 | async-start | bytes 1769472 | tf_op jit(solution)/shard_map/all_gather | solution.py:78
  7.6 11.0 %collective-permute-start = (bf16[768,128]{1,0:T(8,128)(2,1)S(1)}, bf16[768,128]{1,0:T(8,128)(2,1)S(1)}, u32[]{:S(2)}, u32[]{:S(2)}) collective-permute-start(bf16[768,128]{1,0:T(8,128)(2,1)S(1)} %constant_dynamic-slice_fusion.1), channel_id=1, source_target_pairs={{0,4},{4,8},{8,12},{12,16},{16,20},{20,24},{24,28},{28,0},{1,5},{5... | collective-permute-start | bytes 589832 | tf_op jit(solution)/shard_map/ppermute | solution.py:81
  12.1 42.9 %copy-start.11 = (f32[128]{0:T(128)S(1)}, f32[128]{0:T(128)}, u32[]{:S(2)}) copy-start(f32[128]{0:T(128)} %param.17) | copy-start | bytes 1540
  18.6 8.8 %collective-permute-start.1 = (bf16[768,128]{1,0:T(8,128)(2,1)S(1)}, bf16[768,128]{1,0:T(8,128)(2,1)S(1)}, u32[]{:S(2)}, u32[]{:S(2)}) collective-permute-start(bf16[768,128]{1,0:T(8,128)(2,1)S(1)} %collective-permute-done), channel_id=1, source_target_pairs={{0,4},{4,8},{8,12},{12,16},{16,20},{20,24},{24,28},{28,0},{1,5},{5... | collective-permute-start | bytes 589832 | tf_op jit(solution)/shard_map/ppermute | solution.py:81
  27.3 8.4 %collective-permute-start.2 = (bf16[768,128]{1,0:T(8,128)(2,1)S(1)}, bf16[768,128]{1,0:T(8,128)(2,1)S(1)}, u32[]{:S(2)}, u32[]{:S(2)}) collective-permute-start(bf16[768,128]{1,0:T(8,128)(2,1)S(1)} %collective-permute-done.1), channel_id=1, source_target_pairs={{0,4},{4,8},{8,12},{12,16},{16,20},{20,24},{24,28},{28,0},{1,5},{5... | collective-permute-start | bytes 589832 | tf_op jit(solution)/shard_map/ppermute | solution.py:81
  35.7 21.9 %copy-start.5 = (bf16[768,128]{1,0:T(8,128)(2,1)}, bf16[768,128]{1,0:T(8,128)(2,1)S(1)}, u32[]{:S(2)}) copy-start(bf16[768,128]{1,0:T(8,128)(2,1)S(1)} %collective-permute-done.2) | copy-start | bytes 589828
  35.7 8.4 %collective-permute-start.3 = (bf16[768,128]{1,0:T(8,128)(2,1)S(1)}, bf16[768,128]{1,0:T(8,128)(2,1)S(1)}, u32[]{:S(2)}, u32[]{:S(2)}) collective-permute-start(bf16[768,128]{1,0:T(8,128)(2,1)S(1)} %collective-permute-done.2), channel_id=1, source_target_pairs={{0,4},{4,8},{8,12},{12,16},{16,20},{20,24},{24,28},{28,0},{1,5},{5... | collective-permute-start | bytes 589832 | tf_op jit(solution)/shard_map/ppermute | solution.py:81
  36.5 146.2 %reduce-scatter.3.cloned.1.call-start = ((), (), s32[]{:S(2)}) async-start(), calls=%async_computation.2 | async-start | bytes 3932160 | tf_op jit(solution)/shard_map/reduce_scatter | solution.py:118
  44.1 19.5 %copy-start.7 = (bf16[768,128]{1,0:T(8,128)(2,1)}, bf16[768,128]{1,0:T(8,128)(2,1)S(1)}, u32[]{:S(2)}) copy-start(bf16[768,128]{1,0:T(8,128)(2,1)S(1)} %collective-permute-done.3) | copy-start | bytes 589828
  44.1 10.9 %collective-permute-start.4 = (bf16[768,128]{1,0:T(8,128)(2,1)S(1)}, bf16[768,128]{1,0:T(8,128)(2,1)S(1)}, u32[]{:S(2)}, u32[]{:S(2)}) collective-permute-start(bf16[768,128]{1,0:T(8,128)(2,1)S(1)} %collective-permute-done.3), channel_id=1, source_target_pairs={{0,4},{4,8},{8,12},{12,16},{16,20},{20,24},{24,28},{28,0},{1,5},{5... | collective-permute-start | bytes 589832 | tf_op jit(solution)/shard_map/ppermute | solution.py:81
  54.9 8.6 %copy-start.9 = (bf16[768,128]{1,0:T(8,128)(2,1)}, bf16[768,128]{1,0:T(8,128)(2,1)S(1)}, u32[]{:S(2)}) copy-start(bf16[768,128]{1,0:T(8,128)(2,1)S(1)} %collective-permute-done.4) | copy-start | bytes 589828
  54.9 8.6 %collective-permute-start.5 = (bf16[768,128]{1,0:T(8,128)(2,1)S(1)}, bf16[768,128]{1,0:T(8,128)(2,1)}, u32[]{:S(2)}, u32[]{:S(2)}) collective-permute-start(bf16[768,128]{1,0:T(8,128)(2,1)S(1)} %collective-permute-done.4), channel_id=1, source_target_pairs={{0,4},{4,8},{8,12},{12,16},{16,20},{20,24},{24,28},{28,0},{1,5},{5... | collective-permute-start | bytes 589832 | tf_op jit(solution)/shard_map/ppermute | solution.py:81
  63.5 10.2 %collective-permute-start.6 = (bf16[768,128]{1,0:T(8,128)(2,1)}, bf16[768,128]{1,0:T(8,128)(2,1)}, u32[]{:S(2)}, u32[]{:S(2)}) collective-permute-start(bf16[768,128]{1,0:T(8,128)(2,1)} %collective-permute-done.5), channel_id=1, source_target_pairs={{0,4},{4,8},{8,12},{12,16},{16,20},{20,24},{24,28},{28,0},{1,5},{5... | collective-permute-start | bytes 589832 | tf_op jit(solution)/shard_map/ppermute | solution.py:81
  64.9 13.6 %copy-start.4 = (bf16[768,256]{1,0:T(8,128)(2,1)S(1)}, bf16[768,256]{1,0:T(8,128)(2,1)}, u32[]{:S(2)}) copy-start(bf16[768,256]{1,0:T(8,128)(2,1)} %param.16) | copy-start | bytes 1179652
  66.1 14.5 %copy-start.8 = (bf16[768,128]{1,0:T(8,128)(2,1)S(1)}, bf16[768,128]{1,0:T(8,128)(2,1)}, u32[]{:S(2)}) copy-start(bf16[768,128]{1,0:T(8,128)(2,1)} %copy-done.7) | copy-start | bytes 589828
  66.1 14.6 %copy-start.6 = (bf16[768,128]{1,0:T(8,128)(2,1)S(1)}, bf16[768,128]{1,0:T(8,128)(2,1)}, u32[]{:S(2)}) copy-start(bf16[768,128]{1,0:T(8,128)(2,1)} %copy-done.5) | copy-start | bytes 589828
  66.2 14.4 %copy-start.10 = (bf16[768,128]{1,0:T(8,128)(2,1)S(1)}, bf16[768,128]{1,0:T(8,128)(2,1)}, u32[]{:S(2)}) copy-start(bf16[768,128]{1,0:T(8,128)(2,1)} %copy-done.9) | copy-start | bytes 589828
  92.6 8.2 %copy-start.1 = (f32[2048,1536]{1,0:T(8,128)S(1)}, f32[2048,1536]{1,0:T(8,128)}, u32[]{:S(2)}) copy-start(f32[2048,1536]{1,0:T(8,128)} %get-tuple-element.236) | copy-start | bytes 37748740 | tf_op jit(solution)/shard_map/while
  111.8 8.2 %copy-start.1 = (f32[2048,1536]{1,0:T(8,128)S(1)}, f32[2048,1536]{1,0:T(8,128)}, u32[]{:S(2)}) copy-start(f32[2048,1536]{1,0:T(8,128)} %get-tuple-element.236) | copy-start | bytes 37748740 | tf_op jit(solution)/shard_map/while
  131.0 8.2 %copy-start.1 = (f32[2048,1536]{1,0:T(8,128)S(1)}, f32[2048,1536]{1,0:T(8,128)}, u32[]{:S(2)}) copy-start(f32[2048,1536]{1,0:T(8,128)} %get-tuple-element.236) | copy-start | bytes 37748740 | tf_op jit(solution)/shard_map/while
  146.0 36.7 %copy-start.2 = (bf16[768,512]{1,0:T(8,128)(2,1)S(1)}, bf16[768,512]{1,0:T(8,128)(2,1)}, u32[]{:S(2)}) copy-start(bf16[768,512]{1,0:T(8,128)(2,1)} %param.13) | copy-start | bytes 2359300
  146.0 131.2 %all-gather.9.cloned.1.call-start = ((), (), s32[]{:S(2)}) async-start(), calls=%async_computation.4 | async-start | bytes 6488064 | tf_op jit(solution)/shard_map/all_gather | solution.py:128
  146.8 158.6 %all-gather.7.cloned.1.call-start = ((), (), s32[]{:S(2)}) async-start(), calls=%async_computation.3 | async-start | bytes 3932160 | tf_op jit(solution)/shard_map/all_gather | solution.py:125
  192.3 207.5 %all-gather.11.cloned.1.call-start = ((), (), s32[]{:S(2)}) async-start(), calls=%async_computation.5 | async-start | bytes 6488064 | tf_op jit(solution)/shard_map/all_gather | solution.py:133
  192.9 300.1 %all-gather.13.cloned.1.call-start = ((), (), s32[]{:S(2)}) async-start(), calls=%async_computation.6 | async-start | bytes 6488064 | tf_op jit(solution)/shard_map/all_gather | solution.py:139
  193.5 352.4 %reduce-scatter.5.cloned.1.call-start = ((), (), s32[]{:S(2)}) async-start(), calls=%async_computation.7 | async-start | bytes 3932160 | tf_op jit(solution)/shard_map/reduce_scatter | solution.py:142
  509.8 36.1 %copy-start.3 = (bf16[768,512]{1,0:T(8,128)(2,1)S(1)}, bf16[768,512]{1,0:T(8,128)(2,1)}, u32[]{:S(2)}) copy-start(bf16[768,512]{1,0:T(8,128)(2,1)} %reduce-scatter.3.cloned.1.call-done) | copy-start | bytes 2359300
Sparse Core Ops, SparseCore 0:
  36.6 48.5 all-gather.14
  146.2 36.4 reduce-scatter.2
  184.9 92.2 all-gather.8
  278.6 26.6 all-gather.6
  307.4 92.3 all-gather.10
  401.6 91.3 all-gather.12
  509.9 35.8 reduce-scatter.4
